TPU v7x, 32 devices: a whole 2x2x4 slice. The times are simulated.
32 devices in a mesh: sp: 8 (over z, x), tp: 4 (over y, core).
Axes of the slice: x: 2, y: 2, z: 4, core: 2. Of those that a mesh axis runs over, the one named last changes fastest.
Arguments:
- layer_input: bfloat16 [4, 2048, 2048], P(None, ('sp', 'tp')), as said below
- key_weight: bfloat16 [2048, 384], replicated, may hold values from -0.125 to 0.125
- value_weight: bfloat16 [2048, 384], replicated, may hold values from -0.125 to 0.125
- queries: bfloat16 [24, 5, 64], P('sp'), may hold values from -6 to 6
- head_bias: float32 [6, 5], replicated, as said below
Outputs:
- stored: bfloat16 [24, 8, 256, 128], P('sp', None, 'tp')
- first_read: bfloat16 [24, 320], P('sp')
Inputs may be any that keep to these rules, and one draw needn't show every extreme that they name: `layer_input`: entries lie between -12.5 and 12.5. `head_bias`: entries lie between -1 minus the natural logarithm of 2048 and -3.
All inputs are finite; a program needn't handle non-finite values.
Results may differ from a plain program's by a relative error of at most 0.01.
Values may be sent and summed in bfloat16 or wider, within the bound.
A program may use at most 64 MiB of HBM per device.

v0:
```python
import math

import jax
import jax.numpy as jnp
from jax import lax
from jax.sharding import PartitionSpec as P

HD = 64
KVH = 6
GROUP = 5


EPS_NORM = 0.0001


def head_norm(summed):
    squares = jnp.mean(summed * summed, axis=-1, keepdims=True)
    return summed * lax.rsqrt(squares + EPS_NORM)


def shift_table(pair_ids, head_bias):
    heads_range = jnp.arange(KVH, dtype=jnp.int32)
    picker = (pair_ids[:, None] % KVH == heads_range[None, :]).astype(jnp.float32)
    return jnp.dot(picker, head_bias, precision=lax.Precision.HIGHEST)


def per_device(layer_input, key_weight, value_weight, queries, head_bias):
    seq_count, positions, model_width = layer_input.shape
    tokens_flat = layer_input.reshape(seq_count * positions, model_width)
    key_rows = (
        jnp.dot(tokens_flat, key_weight, preferred_element_type=jnp.float32)
        .astype(jnp.bfloat16)
        .reshape(seq_count, positions, KVH, HD)
    )
    value_rows = (
        jnp.dot(tokens_flat, value_weight, preferred_element_type=jnp.float32)
        .astype(jnp.bfloat16)
        .reshape(seq_count, positions, KVH, HD)
    )
    kv_rows = (
        jnp.concatenate([key_rows, value_rows], axis=-1)
        .transpose(0, 2, 1, 3)
        .reshape(seq_count * KVH, 1, positions, 2 * HD)
    )
    stored = lax.all_to_all(kv_rows, "sp", split_axis=0, concat_axis=1, tiled=True)
    score_scale = 1.0 / math.sqrt(HD)
    local_pairs = queries.shape[0]
    pair_ids = lax.axis_index("sp") * local_pairs + jnp.arange(local_pairs, dtype=jnp.int32)
    head_shift = shift_table(pair_ids, head_bias)
    scores = (
        jnp.einsum("pgc,pbtc->pgbt", queries, stored[..., :HD], preferred_element_type=jnp.float32)
        * score_scale
        + head_shift[:, :, None, None]
    )
    keep_log = jax.nn.log_sigmoid(-scores)
    totals = jnp.sum(keep_log, axis=3)
    gathered = lax.all_gather(totals[None], "tp", axis=0, tiled=True)
    later_mask = (jnp.arange(gathered.shape[0], dtype=jnp.int32) > lax.axis_index("tp")).astype(
        jnp.float32
    )
    later_inside = jnp.sum(gathered * later_mask[:, None, None, None], axis=0)
    block_sums = jnp.sum(gathered, axis=0)
    later_blocks = lax.cumsum(block_sums, axis=2, reverse=True) - block_sums
    suffix_log = (
        lax.cumsum(keep_log, axis=3, reverse=True)
        - keep_log
        + (later_inside + later_blocks)[..., None]
    )
    weights = jnp.exp(jax.nn.log_sigmoid(scores) + suffix_log).astype(jnp.bfloat16)
    partial_value = jnp.einsum(
        "pgbt,pbtc->pgc", weights, stored[..., HD:], preferred_element_type=jnp.float32
    )
    summed = lax.psum(partial_value, "tp")
    first_read = head_norm(summed).reshape(local_pairs, GROUP * HD).astype(jnp.bfloat16)
    return (stored, first_read)


def solution(mesh):
    in_specs = (P(None, ("sp", "tp"), None), P(), P(), P("sp", None, None), P())
    out_specs = (P("sp", None, "tp", None), P("sp", None))
    return jax.shard_map(
        per_device, mesh=mesh, in_specs=in_specs, out_specs=out_specs, check_vma=False
    )
```

profile of v0, /device:TPU:0, one launch (start us, length us, event | category | flops | bytes accessed | tf_op | source)
XLA Modules:
  0.0 53.3 jit_solution(13283465844717739790)
XLA Ops:
  0.6 0.0 copy-start
  0.6 1.4 %copy-done = bf16[2048,384]{1,0:T(8,128)(2,1)S(1)} copy-done((bf16[2048,384]{1,0:T(8,128)(2,1)S(1)}, bf16[2048,384]{1,0:T(8,128)(2,1)}, u32[]{:S(2)}) %copy-start) | copy-done | bytes 1572888
  2.0 0.0 copy-start.2
  2.0 2.0 %convolution_convert_fusion.1 = bf16[256,384]{1,0:T(8,128)(2,1)S(1)} fusion(bf16[256,2048]{1,0:T(8,128)(2,1)} %bitcast.33, bf16[2048,384]{1,0:T(8,128)(2,1)S(1)} %copy-done), kind=kOutput, calls=%fused_computation.1 | convolution fusion | flops 402751488 | bytes 2818048 | tf_op jit(solution)/shard_map/dot_general | solution.py:31
  4.1 0.1 copy.26
  4.2 0.2 reshape.69
  4.4 0.0 copy-done.2
  4.4 2.1 %convolution_convert_fusion = bf16[256,384]{1,0:T(8,128)(2,1)S(1)} fusion(bf16[256,2048]{1,0:T(8,128)(2,1)S(1)} %bitcast.34, bf16[2048,384]{1,0:T(8,128)(2,1)} %param.7), kind=kOutput, calls=%fused_computation | convolution fusion | flops 402751488 | bytes 2818048 | tf_op jit(solution)/shard_map/dot_general | solution.py:36
  6.6 0.1 copy.27
  6.7 0.2 reshape.70
  6.9 0.0 copy-start.4
  6.9 0.6 %maximum_bitcast_fusion = bf16[4,6,64,128]{2,0,3,1:T(4,128)(2,1)S(1)} fusion(bf16[4,64,6,64]{1,0,3,2:T(4,128)(2,1)S(1)} %reshape.70, bf16[4,64,6,64]{1,0,3,2:T(4,128)(2,1)S(1)} %reshape.69), kind=kLoop, calls=%fused_computation.6 | loop fusion | flops 196608 | bytes 786432 | tf_op jit(solution)/shard_map/transpose | solution.py:42
  7.6 0.0 copy-start.3
  7.6 1.2 %copy.28 = bf16[4,6,64,128]{3,2,1,0:T(8,128)(2,1)} copy(bf16[4,6,64,128]{2,0,3,1:T(4,128)(2,1)S(1)} %maximum_bitcast_fusion) | data formatting | bytes 786432 | tf_op jit(solution)/shard_map/transpose | solution.py:42
  8.7 7.3 %all-to-all-start = ((bf16[24,1,64,128]{3,2,1,0:T(8,128)(2,1)}), bf16[24,1,64,128]{3,2,1,0:T(8,128)(2,1)S(1)}, u32[]{:S(2)}, u32[]{:S(2)}) async-start(bf16[24,1,64,128]{3,2,1,0:T(8,128)(2,1)} %bitcast.3), calls=%async_computation | async-start | bytes 786432 | tf_op jit(solution)/shard_map/all_to_all | solution.py:45
  16.0 0.0 copy-done.4
  16.1 0.2 fusion.15
  16.2 11.5 %all-to-all-done = bf16[24,1,64,128]{3,2,1,0:T(8,128)(2,1)S(1)} async-done(((bf16[24,1,64,128]{3,2,1,0:T(8,128)(2,1)}), bf16[24,1,64,128]{3,2,1,0:T(8,128)(2,1)S(1)}, u32[]{:S(2)}, u32[]{:S(2)}) %all-to-all-start) | async-done | bytes 393248 | tf_op jit(solution)/shard_map/all_to_all | solution.py:45
  27.7 0.0 copy-start.1
  27.7 0.0 copy-done.3
  27.8 0.5 fusion.9
  28.3 0.1 copy.34
  28.4 5.2 %all-gather = f32[12,5,8]{2,1,0:T(8,128)S(1)} all-gather(f32[3,5,8]{2,1,0:T(8,128)S(1)} %copy.34), channel_id=2, replica_groups=mesh['sp'=8,'tp'=4] {'tp'}, dimensions={0}, use_global_device_ids=true | all-gather | bytes 2400 | tf_op jit(solution)/shard_map/all_gather | solution.py:57
  33.6 0.1 fusion.19
  33.7 0.5 reduce_window_sum.21
  34.2 0.1 copy.35
  34.3 6.4 %reduce_window_sum.20 = f32[3,5,8,64]{3,2,1,0:T(8,128)S(1)} reduce-window(f32[3,5,8,64]{3,2,1,0:T(8,128)S(1)} %copy.32, f32[]{:T(128)} %constant.36.clone.1), window={size=1x1x1x64 pad=0_0x0_0x0_0x0_63}, to_apply=%region_0.1 | reduce-window | flops 483840 | bytes 61444 | tf_op jit(solution)/shard_map/per_device/reduce_window_sum | solution.py:65
  40.7 0.4 convolution_bitcast_fusion
  41.1 11.4 %psum.7 = f32[3,5,64]{2,1,0:T(8,128)S(1)} all-reduce(f32[3,5,64]{2,1,0:T(8,128)S(1)} %convolution_bitcast_fusion), channel_id=1, replica_groups=mesh['sp'=8,'tp'=4] {'tp'}, use_global_device_ids=true, to_apply=%region_5.6 | all-reduce | flops 960 | bytes 7680 | tf_op jit(solution)/shard_map/psum | solution.py:73
  52.5 0.1 multiply_reduce_fusion.1
  52.6 0.1 multiply_convert_fusion
  52.7 0.7 %convert_element_type.28 = bf16[3,320]{1,0:T(4,128)(2,1)} reshape(bf16[3,5,64]{2,1,0:T(8,128)(2,1)S(1)} %multiply_convert_fusion) | data formatting | bytes 3840 | tf_op jit(solution)/shard_map/convert_element_type | solution.py:74
  53.3 0.0 copy-done.1
  (7 shorter events, 0.1 us)
Async XLA Ops:
  0.6 1.4 %copy-start = (bf16[2048,384]{1,0:T(8,128)(2,1)S(1)}, bf16[2048,384]{1,0:T(8,128)(2,1)}, u32[]{:S(2)}) copy-start(bf16[2048,384]{1,0:T(8,128)(2,1)} %param.6) | copy-start | bytes 4718596
  2.0 2.4 %copy-start.2 = (bf16[4,64,2048]{2,1,0:T(8,128)(2,1)S(1)}, bf16[4,64,2048]{2,1,0:T(8,128)(2,1)}, u32[]{:S(2)}) copy-start(bf16[4,64,2048]{2,1,0:T(8,128)(2,1)} %param.5) | copy-start | bytes 3145732
  6.9 9.1 %copy-start.4 = (f32[6,5]{1,0:T(8,128)S(1)}, f32[6,5]{1,0:T(8,128)}, u32[]{:S(2)}) copy-start(f32[6,5]{1,0:T(8,128)} %param.9) | copy-start | bytes 364
  7.6 20.2 %copy-start.3 = (bf16[3,5,64]{2,0,1:T(4,128)(2,1)S(1)}, bf16[3,5,64]{2,0,1:T(4,128)(2,1)}, u32[]{:S(2)}) copy-start(bf16[3,5,64]{2,0,1:T(4,128)(2,1)} %param.8) | copy-start | bytes 5764
  8.7 19.0 %all-to-all-start = ((bf16[24,1,64,128]{3,2,1,0:T(8,128)(2,1)}), bf16[24,1,64,128]{3,2,1,0:T(8,128)(2,1)S(1)}, u32[]{:S(2)}, u32[]{:S(2)}) async-start(bf16[24,1,64,128]{3,2,1,0:T(8,128)(2,1)} %bitcast.3), calls=%async_computation | async-start | bytes 786432 | tf_op jit(solution)/shard_map/all_to_all | solution.py:45
  27.7 25.6 %copy-start.1 = (bf16[8,3,1,64,128]{4,3,0,1,2:T(8,128)(2,1)}, bf16[8,3,1,64,128]{4,3,0,1,2:T(8,128)(2,1)S(1)}, u32[]{:S(2)}) copy-start(bf16[8,3,1,64,128]{4,3,0,1,2:T(8,128)(2,1)S(1)} %copy.51) | copy-start | bytes 1179652
where the time goes:
time: 53.7 us; the launch traced here: 53.3 us
  blocking collectives  16.6 us (31%)
  waiting for transfers between devices  11.5 us (21%)
  other arithmetic  7.8 us (15%)
  starting transfers between devices  7.28 us (14%)
  matrix products  5.23 us (10%)
  local copies, waits for them, and re-layouts  4.2 us (8%)
  between operations  0.75 us (1%)
    all_to_all x1, waiting for transfers between devices, per_device(): lax.all_to_all(kv_rows, 'sp', split_axis=0, concat_axis=1, tiled=True)  11.5 us
    psum x1, blocking collectives, per_device(): summed = lax.psum(partial_value, 'tp')  11.4 us
    all_to_all x1, starting transfers between devices, per_device(): lax.all_to_all(kv_rows, 'sp', split_axis=0, concat_axis=1, tiled=True)  7.28 us
    another operation x1, other arithmetic, per_device(): lax.cumsum(keep_log, axis=3, reverse=True) - keep_log  6.41 us
    all_gather x1, blocking collectives, per_device(): gathered = lax.all_gather(totals[None], 'tp', axis=0, tiled=True)  5.21 us
    dot_general x1, matrix products, per_device(): jnp.dot(tokens_flat, value_weight, preferred_element_type=jnp.float32)  2.12 us
    dot_general x1, matrix products, per_device(): jnp.dot(tokens_flat, key_weight, preferred_element_type=jnp.float32)  2.02 us
    unnamed x10, local copies, waits for them, and re-layouts  1.43 us
  transfers between devices with their start and end apart: 1, of which 1 were waited for; matrix products, arithmetic and copies ran while one was open for 0% of the time, Pallas kernels for 0%

commit v1 on v0

v1 whole, which is shorter than its diff:
```python
import functools
import math

import jax
import jax.numpy as jnp
from jax import lax
from jax.experimental import pallas as pl
from jax.experimental.pallas import tpu as pltpu
from jax.sharding import PartitionSpec as P

EPS_NORM = 0.0001
MESH = pl.DeviceIdType.MESH
KC = 4
ROWS = 8


def flip(index, k):
    bit = 1
    while bit <= k:
        if k & bit:
            index = index + (1 - 2 * ((index // bit) % 2)) * bit
        bit *= 2
    return index


def kernel(
    sp, tp, seqs, sub, hd, kvh, group, pairs,
    x_hbm, wk_hbm, wv_hbm, q_hbm, bias_hbm,
    stored_hbm, first_ref,
    x_v, wk_v, wv_v, q_v, bias_v, send, recv, msg, fin,
    x_sem, w_sem, small_sem, send_sem, recv_sem, msend_sem, mrecv_sem, out_sem,
):
    me = lax.axis_index("sp")
    mt = lax.axis_index("tp")
    per_seq = kvh // pairs
    width = x_hbm.shape[1]
    kc = width // KC
    half_rows = seqs * sub // 2

    barrier = pltpu.get_barrier_semaphore()
    for k in range(1, sp):
        pl.semaphore_signal(barrier, inc=1, device_id={"sp": flip(me, k)}, device_id_type=MESH)
    for k in range(1, tp):
        pl.semaphore_signal(barrier, inc=1, device_id={"tp": lax.rem(mt + k, tp)}, device_id_type=MESH)

    top = me // (sp // 2)
    far_row = pl.multiple_of((1 - top) * half_rows, half_rows)
    near_row = pl.multiple_of(top * half_rows, half_rows)

    x_far = pltpu.make_async_copy(x_hbm.at[pl.ds(far_row, half_rows)], x_v.at[pl.ds(far_row, half_rows)], x_sem.at[0])
    x_near = pltpu.make_async_copy(x_hbm.at[pl.ds(near_row, half_rows)], x_v.at[pl.ds(near_row, half_rows)], x_sem.at[1])
    x_far.start()
    w_copies = []
    for c in range(KC):
        rows = pl.ds(c * kc, kc)
        a = pltpu.make_async_copy(wk_hbm.at[rows], wk_v.at[rows], w_sem.at[0, c])
        b = pltpu.make_async_copy(wv_hbm.at[rows], wv_v.at[rows], w_sem.at[1, c])
        a.start()
        b.start()
        w_copies.append((a, b))
    x_near.start()
    q_copy = pltpu.make_async_copy(q_hbm, q_v, small_sem.at[0])
    bias_copy = pltpu.make_async_copy(bias_hbm, bias_v, small_sem.at[1])
    q_copy.start()
    bias_copy.start()

    def project(row0):
        return project_cols(row0)

    def pieces(keys, values, i, part):
        out = []
        for p in range(pairs):
            c0 = (part * pairs + p) * hd
            out.append(keys[i * sub:(i + 1) * sub, c0:c0 + hd])
            out.append(values[i * sub:(i + 1) * sub, c0:c0 + hd])
        return jnp.concatenate(out, axis=1).astype(jnp.bfloat16)

    x_far.wait()
    keys = values = None
    for c in range(KC):
        w_copies[c][0].wait()
        w_copies[c][1].wait()
        xc = x_v[pl.ds(far_row, half_rows), c * kc:(c + 1) * kc]
        dk = jnp.dot(xc, wk_v[c * kc:(c + 1) * kc, :], preferred_element_type=jnp.float32)
        dv = jnp.dot(xc, wv_v[c * kc:(c + 1) * kc, :], preferred_element_type=jnp.float32)
        keys = dk if keys is None else keys + dk
        values = dv if values is None else values + dv
    far_base = (1 - top) * (sp // 2)
    for i in range(seqs // 2):
        for part in range(per_seq):
            send[pl.ds(far_base + i * per_seq + part, 1)] = pieces(keys, values, i, part)[None]

    pl.semaphore_wait(barrier, sp + tp - 2)

    def block_copy(k):
        to = flip(me, k)
        return pltpu.make_async_remote_copy(
            src_ref=send.at[to], dst_ref=recv.at[me],
            send_sem=send_sem.at[to], recv_sem=recv_sem.at[me],
            device_id={"sp": to}, device_id_type=MESH,
        )

    def arrived(k):
        frm = flip(me, k)
        return pltpu.make_async_remote_copy(
            src_ref=send.at[frm], dst_ref=recv.at[frm],
            send_sem=send_sem.at[frm], recv_sem=recv_sem.at[frm],
            device_id={"sp": frm}, device_id_type=MESH,
        )

    for k in range(sp // 2, sp):
        block_copy(k).start()

    x_near.wait()
    xn = x_v[pl.ds(near_row, half_rows), :]
    keys = jnp.dot(xn, wk_v[...], preferred_element_type=jnp.float32)
    values = jnp.dot(xn, wv_v[...], preferred_element_type=jnp.float32)
    near_base = top * (sp // 2)
    for i in range(seqs // 2):
        for part in range(per_seq):
            send[pl.ds(near_base + i * per_seq + part, 1)] = pieces(keys, values, i, part)[None]
    for k in range(1, sp // 2):
        block_copy(k).start()
    recv[pl.ds(me, 1)] = send[pl.ds(me, 1)]

    q_copy.wait()
    bias_copy.wait()
    h0 = lax.rem(me * pairs, kvh)
    eye = lax.broadcasted_iota(jnp.int32, (ROWS, group), 0) == lax.broadcasted_iota(jnp.int32, (ROWS, group), 1)
    q_pads = []
    shifts = []
    for p in range(pairs):
        qp = q_v[p].astype(jnp.float32)
        qp = jnp.concatenate([qp, jnp.zeros((group, hd), jnp.float32)], axis=1)
        qp = jnp.concatenate([qp, jnp.zeros((ROWS - group, 2 * hd), jnp.float32)], axis=0)
        q_pads.append(qp.astype(jnp.bfloat16))
        row = bias_v[pl.ds(h0 + p, 1), :]
        shifts.append(jnp.sum(jnp.where(eye, jnp.broadcast_to(row, (ROWS, group)), 0.0), axis=1, keepdims=True))
    shift = jnp.concatenate(shifts, axis=0)
    scale = 1.0 / math.sqrt(hd)
    later = lax.broadcasted_iota(jnp.int32, (sub, 256), 0)
    column = lax.broadcasted_iota(jnp.int32, (sub, 256), 1)
    tri = ((later > column) | (column >= 128)).astype(jnp.float32).astype(jnp.bfloat16)
    left_half = lax.broadcasted_iota(jnp.int32, (pairs * ROWS, 2 * hd), 1) < hd

    def msg_copy(b, t):
        return pltpu.make_async_remote_copy(
            src_ref=msg.at[mt, b], dst_ref=msg.at[mt, b],
            send_sem=msend_sem.at[t, b], recv_sem=mrecv_sem.at[mt, b],
            device_id={"tp": t}, device_id_type=MESH,
        )

    def msg_arrived(b, t):
        return pltpu.make_async_remote_copy(
            src_ref=msg.at[t, b], dst_ref=msg.at[t, b],
            send_sem=msend_sem.at[t, b], recv_sem=mrecv_sem.at[t, b],
            device_id={"tp": t}, device_id_type=MESH,
        )

    def out_copies(b):
        return [
            pltpu.make_async_copy(recv.at[b, :, pl.ds(p * 2 * hd, 2 * hd)], stored_hbm.at[p, b], out_sem.at[b, p])
            for p in range(pairs)
        ]

    def attend(b):
        scores = []
        for p in range(pairs):
            kv = recv[b, :, p * 2 * hd:(p + 1) * 2 * hd]
            scores.append(lax.dot_general(q_pads[p], kv, (((1,), (1,)), ((), ())), preferred_element_type=jnp.float32))
        s = jnp.concatenate(scores, axis=0) * scale + shift
        low = jnp.log1p(jnp.exp(-jnp.abs(s)))
        keep = -(jnp.maximum(s, 0.0) + low)
        sig = jnp.minimum(s, 0.0) - low
        hi = keep.astype(jnp.bfloat16)
        rest = keep - hi.astype(jnp.float32)
        mid = rest.astype(jnp.bfloat16)
        lo = (rest - mid.astype(jnp.float32)).astype(jnp.bfloat16)
        n = pairs * ROWS
        sums = (
            jnp.dot(hi, tri, preferred_element_type=jnp.float32)
            + jnp.dot(mid, tri, preferred_element_type=jnp.float32)
            + jnp.dot(lo, tri, preferred_element_type=jnp.float32)
        )
        weights = jnp.exp(sig + sums[:, :sub]).astype(jnp.bfloat16)
        reads = []
        for p in range(pairs):
            kv = recv[b, :, p * 2 * hd:(p + 1) * 2 * hd]
            reads.append(jnp.dot(weights[p * ROWS:(p + 1) * ROWS], kv, preferred_element_type=jnp.float32))
        read = jnp.concatenate(reads, axis=0)
        msg[mt, b] = jnp.where(left_half, sums[:, 128:128 + 2 * hd], read)
        for t in range(1, tp):
            msg_copy(b, lax.rem(mt + t, tp)).start()

    order = [0] + list(range(1, sp))
    for k in order:
        b = flip(me, k)
        if k:
            arrived(k).wait_recv()
        for copy in out_copies(b):
            copy.start()
        attend(b)

    for b in range(sp):
        for t in range(1, tp):
            msg_arrived(b, lax.rem(mt + t, tp)).wait_recv()

    def add_block(i, carry):
        total, acc = carry
        b = sp - 1 - i
        for j in range(tp - 1, -1, -1):
            m = msg[j, b]
            total = total + jnp.exp(acc) * m
            acc = acc + pltpu.roll(m, hd, 1)
        return total, acc

    zero = jnp.zeros((pairs * ROWS, 2 * hd), jnp.float32)
    total, _ = lax.fori_loop(0, sp, add_block, (zero, zero), unroll=True)
    total = jnp.where(left_half, 0.0, total)
    squares = jnp.sum(total * total, axis=1, keepdims=True) * (1.0 / hd)
    fin[...] = pltpu.roll(total * lax.rsqrt(squares + EPS_NORM), hd, 1)
    cols = [fin[pl.ds(g, pairs, stride=ROWS), :][:, :hd] for g in range(group)]
    first_ref[...] = jnp.concatenate(cols, axis=1).astype(first_ref.dtype)

    for k in range(1, sp):
        block_copy(k).wait_send()
    for b in range(sp):
        for t in range(1, tp):
            msg_copy(b, lax.rem(mt + t, tp)).wait_send()
        for copy in out_copies(b):
            copy.wait()


def solution(mesh):
    sp, tp = mesh.shape["sp"], mesh.shape["tp"]

    def per_device(layer_input, key_weight, value_weight, queries, head_bias):
        seqs, sub, width = layer_input.shape
        pairs, group, hd = queries.shape
        kvh = head_bias.shape[0]
        x = layer_input.reshape(seqs * sub, width)
        block = pairs * 2 * hd
        any_spec = pl.BlockSpec(memory_space=pl.ANY)
        dma = pltpu.SemaphoreType.DMA
        stored, first = pl.pallas_call(
            functools.partial(kernel, sp, tp, seqs, sub, hd, kvh, group, pairs),
            out_shape=(
                jax.ShapeDtypeStruct((pairs, sp, sub, 2 * hd), jnp.bfloat16),
                jax.ShapeDtypeStruct((pairs, group * hd), jnp.bfloat16),
            ),
            in_specs=[any_spec] * 5,
            out_specs=(any_spec, pl.BlockSpec(memory_space=pltpu.VMEM)),
            scratch_shapes=[
                pltpu.VMEM(x.shape, jnp.bfloat16),
                pltpu.VMEM(key_weight.shape, jnp.bfloat16),
                pltpu.VMEM(value_weight.shape, jnp.bfloat16),
                pltpu.VMEM(queries.shape, jnp.bfloat16),
                pltpu.VMEM(head_bias.shape, jnp.float32),
                pltpu.VMEM((sp, sub, block), jnp.bfloat16),
                pltpu.VMEM((sp, sub, block), jnp.bfloat16),
                pltpu.VMEM((tp, sp, pairs * ROWS, 2 * hd), jnp.float32),
                pltpu.VMEM((pairs * ROWS, 2 * hd), jnp.float32),
                dma((2,)),
                dma((2, KC)),
                dma((2,)),
                dma((sp,)),
                dma((sp,)),
                dma((tp, sp)),
                dma((tp, sp)),
                dma((sp, pairs)),
            ],
            compiler_params=pltpu.CompilerParams(collective_id=0, has_side_effects=True),
        )(x, key_weight, value_weight, queries, head_bias)
        return stored, first

    in_specs = (P(None, ("sp", "tp"), None), P(), P(), P("sp", None, None), P())
    out_specs = (P("sp", None, "tp", None), P("sp", None))
    return jax.shard_map(per_device, mesh=mesh, in_specs=in_specs, out_specs=out_specs, check_vma=False)
```

time: 53.7 us -> 27.6 us (0.51)
  Pallas kernels: 0 us -> 22.5 us
  blocking collectives: 16.6 us -> 0 us
  waiting for transfers between devices: 11.5 us -> 0 us
  other arithmetic: 7.8 us -> 0 us
  starting transfers between devices: 7.28 us -> 0 us
  matrix products: 5.23 us -> 0 us
    pallas_call x0 -> x1, Pallas kernels: none -> 22.5 us  [per_device(): pl.pallas_call(functools.partial(kernel, sp, tp, seqs, sub, hd, kvh, grou...]
    all_to_all x1 -> x0, waiting for transfers between devices: 11.5 us -> none  [per_device(): lax.all_to_all(kv_rows, 'sp', split_axis=0, concat_axis=1, tiled=True)]
    psum x1 -> x0, blocking collectives: 11.4 us -> none  [per_device(): summed = lax.psum(partial_value, 'tp')]
    all_to_all x1 -> x0, starting transfers between devices: 7.28 us -> none  [per_device(): lax.all_to_all(kv_rows, 'sp', split_axis=0, concat_axis=1, tiled=True)]
    another operation x2 -> x0, other arithmetic: 6.9 us -> none  [the longest x1 6.41 us: per_device(): lax.cumsum(keep_log, axis=3, reverse=True) - keep_log]
    dot_general x5 -> x0, matrix products: 5.23 us -> none  [the longest x1 2.12 us: per_device(): jnp.dot(tokens_flat, value_weight, preferred_element_type=jnp.float32)]
    all_gather x1 -> x0, blocking collectives: 5.21 us -> none  [per_device(): gathered = lax.all_gather(totals[None], 'tp', axis=0, tiled=True)]
    unnamed x10 -> x3, local copies, waits for them, and re-layouts: 1.43 us -> 4.3 us
  transfers between devices with their start and end apart: 1 -> 0, of which waited for: 1 -> 0; matrix products, arithmetic and copies ran while one was open for 0% -> 0% of each run, Pallas kernels for 0% -> 0%
where the time goes in v1:
time: 27.6 us; the launch traced here: 27.4 us
  Pallas kernels  22.5 us (82%)
  local copies, waits for them, and re-layouts  4.3 us (16%)
  between operations  0.64 us (2%)
    pallas_call x1, Pallas kernels, per_device(): pl.pallas_call(functools.partial(kernel, sp, tp, seqs, sub, hd, kvh, grou...  22.5 us
    unnamed x3, local copies, waits for them, and re-layouts  4.3 us

profile of v1, /device:TPU:0, one launch (start us, length us, event | category | flops | bytes accessed | tf_op | source)
XLA Modules:
  0.0 27.4 jit_solution(304546059587650135)
XLA Ops:
  0.6 1.3 %copy.7.q_hbm = bf16[3,5,64]{2,1,0:T(8,128)(2,1)} copy(bf16[3,5,64]{2,0,1:T(4,128)(2,1)} %param.8) | data formatting | bytes 3840 | tf_op args[3]
  1.9 22.5 %shard_map.68 = (bf16[3,8,64,128]{3,2,1,0:T(8,128)(2,1)}, bf16[3,320]{1,0:T(4,128)(2,1)}) custom-call(bf16[256,2048]{1,0:T(8,128)(2,1)} %bitcast.1, bf16[2048,384]{1,0:T(8,128)(2,1)} %wk_hbm.1, bf16[2048,384]{1,0:T(8,128)(2,1)} %wv_hbm.1, bf16[3,5,64]{2,1,0:T(8,128)(2,1)} %copy.7.q_hbm, f32[6,5]{1,0:T(8,128)} %bias_hbm.1), custom_call_target="tpu_custom_call" | custom-call | tf_op jit(solution)/shard_map/pallas_call | solution.py:245
  24.4 1.8 %copy.10 = bf16[3,8,64,128]{3,2,1,0:T(8,128)(2,1)} copy(bf16[3,8,64,128]{3,2,1,0:T(8,128)(2,1)} %get-tuple-element.4) | data formatting | bytes 786432
  26.2 1.3 %copy.11 = bf16[3,320]{1,0:T(4,128)(2,1)} copy(bf16[3,320]{1,0:T(4,128)(2,1)} %get-tuple-element.5) | data formatting | bytes 3840

commit v2 on v1

--- a/solution.py
+++ b/solution.py
@@ -11,6 +11,7 @@
 EPS_NORM = 0.0001
 MESH = pl.DeviceIdType.MESH
 KC = 4
+VMEM_BYTES = 60 * 1024 * 1024
 ROWS = 8
 
 
@@ -26,9 +27,9 @@
 def kernel(
     sp, tp, seqs, sub, hd, kvh, group, pairs,
     x_hbm, wk_hbm, wv_hbm, q_hbm, bias_hbm,
-    stored_hbm, first_ref,
-    x_v, wk_v, wv_v, q_v, bias_v, send, recv, msg, fin,
-    x_sem, w_sem, small_sem, send_sem, recv_sem, msend_sem, mrecv_sem, out_sem,
+    recv, msg,
+    x_v, wk_v, wv_v, q_v, bias_v, send,
+    x_sem, w_sem, small_sem, send_sem, recv_sem, msend_sem, mrecv_sem,
 ):
     me = lax.axis_index("sp")
     mt = lax.axis_index("tp")
@@ -64,9 +65,6 @@
     q_copy.start()
     bias_copy.start()
 
-    def project(row0):
-        return project_cols(row0)
-
     def pieces(keys, values, i, part):
         out = []
         for p in range(pairs):
@@ -130,7 +128,7 @@
     q_pads = []
     shifts = []
     for p in range(pairs):
-        qp = q_v[p].astype(jnp.float32)
+        qp = q_v[:, p, :].astype(jnp.float32)
         qp = jnp.concatenate([qp, jnp.zeros((group, hd), jnp.float32)], axis=1)
         qp = jnp.concatenate([qp, jnp.zeros((ROWS - group, 2 * hd), jnp.float32)], axis=0)
         q_pads.append(qp.astype(jnp.bfloat16))
@@ -156,12 +154,6 @@
             send_sem=msend_sem.at[t, b], recv_sem=mrecv_sem.at[t, b],
             device_id={"tp": t}, device_id_type=MESH,
         )
-
-    def out_copies(b):
-        return [
-            pltpu.make_async_copy(recv.at[b, :, pl.ds(p * 2 * hd, 2 * hd)], stored_hbm.at[p, b], out_sem.at[b, p])
-            for p in range(pairs)
-        ]
 
     def attend(b):
         scores = []
@@ -197,13 +189,28 @@
         b = flip(me, k)
         if k:
             arrived(k).wait_recv()
-        for copy in out_copies(b):
-            copy.start()
         attend(b)
 
     for b in range(sp):
         for t in range(1, tp):
             msg_arrived(b, lax.rem(mt + t, tp)).wait_recv()
+
+    for k in range(1, sp):
+        block_copy(k).wait_send()
+    for b in range(sp):
+        for t in range(1, tp):
+            msg_copy(b, lax.rem(mt + t, tp)).wait_send()
+
+
+def finish(sp, tp, hd, group, pairs, recv, msg, stored_hbm, first_ref, fin, out_sem):
+    copies = [
+        pltpu.make_async_copy(recv.at[b, :, pl.ds(p * 2 * hd, 2 * hd)], stored_hbm.at[p, b], out_sem.at[b, p])
+        for b in range(sp)
+        for p in range(pairs)
+    ]
+    for copy in copies:
+        copy.start()
+    left_half = lax.broadcasted_iota(jnp.int32, (pairs * ROWS, 2 * hd), 1) < hd
 
     def add_block(i, carry):
         total, acc = carry
@@ -222,13 +229,8 @@
     cols = [fin[pl.ds(g, pairs, stride=ROWS), :][:, :hd] for g in range(group)]
     first_ref[...] = jnp.concatenate(cols, axis=1).astype(first_ref.dtype)
 
-    for k in range(1, sp):
-        block_copy(k).wait_send()
-    for b in range(sp):
-        for t in range(1, tp):
-            msg_copy(b, lax.rem(mt + t, tp)).wait_send()
-        for copy in out_copies(b):
-            copy.wait()
+    for copy in copies:
+        copy.wait()
 
 
 def solution(mesh):
@@ -240,26 +242,26 @@
         kvh = head_bias.shape[0]
         x = layer_input.reshape(seqs * sub, width)
         block = pairs * 2 * hd
-        any_spec = pl.BlockSpec(memory_space=pl.ANY)
+        any_spec = pl.BlockSpec(memory_space=pltpu.HBM)
         dma = pltpu.SemaphoreType.DMA
-        stored, first = pl.pallas_call(
+        handed = sp * sub * block * 2 + tp * sp * pairs * ROWS * 2 * hd * 4
+        limit = VMEM_BYTES - handed
+        vmem_spec = pl.BlockSpec(memory_space=pltpu.VMEM)
+        recv, msg = pl.pallas_call(
             functools.partial(kernel, sp, tp, seqs, sub, hd, kvh, group, pairs),
             out_shape=(
-                jax.ShapeDtypeStruct((pairs, sp, sub, 2 * hd), jnp.bfloat16),
-                jax.ShapeDtypeStruct((pairs, group * hd), jnp.bfloat16),
+                pltpu.VMEM((sp, sub, block), jnp.bfloat16),
+                pltpu.VMEM((tp, sp, pairs * ROWS, 2 * hd), jnp.float32),
             ),
             in_specs=[any_spec] * 5,
-            out_specs=(any_spec, pl.BlockSpec(memory_space=pltpu.VMEM)),
+            out_specs=(vmem_spec, vmem_spec),
             scratch_shapes=[
                 pltpu.VMEM(x.shape, jnp.bfloat16),
                 pltpu.VMEM(key_weight.shape, jnp.bfloat16),
                 pltpu.VMEM(value_weight.shape, jnp.bfloat16),
-                pltpu.VMEM(queries.shape, jnp.bfloat16),
+                pltpu.VMEM((group, pairs, hd), jnp.bfloat16),
                 pltpu.VMEM(head_bias.shape, jnp.float32),
                 pltpu.VMEM((sp, sub, block), jnp.bfloat16),
-                pltpu.VMEM((sp, sub, block), jnp.bfloat16),
-                pltpu.VMEM((tp, sp, pairs * ROWS, 2 * hd), jnp.float32),
-                pltpu.VMEM((pairs * ROWS, 2 * hd), jnp.float32),
                 dma((2,)),
                 dma((2, KC)),
                 dma((2,)),
@@ -267,11 +269,25 @@
                 dma((sp,)),
                 dma((tp, sp)),
                 dma((tp, sp)),
+            ],
+            compiler_params=pltpu.CompilerParams(
+                collective_id=0, has_side_effects=True, vmem_limit_bytes=limit
+            ),
+        )(x, key_weight, value_weight, queries.transpose(1, 0, 2), head_bias)
+        return pl.pallas_call(
+            functools.partial(finish, sp, tp, hd, group, pairs),
+            out_shape=(
+                jax.ShapeDtypeStruct((pairs, sp, sub, 2 * hd), jnp.bfloat16),
+                jax.ShapeDtypeStruct((pairs, group * hd), jnp.bfloat16),
+            ),
+            in_specs=[vmem_spec, vmem_spec],
+            out_specs=(any_spec, vmem_spec),
+            scratch_shapes=[
+                pltpu.VMEM((pairs * ROWS, 2 * hd), jnp.float32),
                 dma((sp, pairs)),
             ],
-            compiler_params=pltpu.CompilerParams(collective_id=0, has_side_effects=True),
-        )(x, key_weight, value_weight, queries, head_bias)
-        return stored, first
+            compiler_params=pltpu.CompilerParams(vmem_limit_bytes=VMEM_BYTES // 4),
+        )(recv, msg)
 
     in_specs = (P(None, ("sp", "tp"), None), P(), P(), P("sp", None, None), P())
     out_specs = (P("sp", None, "tp", None), P("sp", None))

time: 27.6 us -> 23.9 us (0.87)
  local copies, waits for them, and re-layouts: 4.3 us -> 0 us
  Pallas kernels: 22.5 us -> 23.1 us
    unnamed x3 -> x0, local copies, waits for them, and re-layouts: 4.3 us -> none
    pallas_call x0 -> x1, Pallas kernels: none -> 1.67 us  [per_device(): pl.pallas_call(functools.partial(finish, sp, tp, hd, group, pairs), out_s...]
    pallas_call x1, Pallas kernels: 22.5 us -> 21.4 us  [per_device(): pl.pallas_call(functools.partial(kernel, sp, tp, seqs, sub, hd, kvh, grou...]
where the time goes in v2:
time: 23.9 us; the launch traced here: 23.7 us
  Pallas kernels  23.1 us (97%)
  between operations  0.64 us (3%)
    pallas_call x1, Pallas kernels, per_device(): pl.pallas_call(functools.partial(kernel, sp, tp, seqs, sub, hd, kvh, grou...  21.4 us
    pallas_call x1, Pallas kernels, per_device(): pl.pallas_call(functools.partial(finish, sp, tp, hd, group, pairs), out_s...  1.67 us

profile of v2, /device:TPU:0, one launch (start us, length us, event | category | flops | bytes accessed | tf_op | source)
XLA Modules:
  0.0 23.7 jit_solution(14775064819835318668)
XLA Ops:
  0.6 21.4 %shard_map.68 = (bf16[8,64,384]{2,1,0:T(8,128)(2,1)S(1)}, f32[4,8,24,128]{3,2,1,0:T(8,128)S(1)}) custom-call(bf16[256,2048]{1,0:T(8,128)(2,1)} %bitcast.2, bf16[2048,384]{1,0:T(8,128)(2,1)} %wk_hbm.1, bf16[2048,384]{1,0:T(8,128)(2,1)} %wv_hbm.1, bf16[5,3,64]{2,1,0:T(4,128)(2,1)} %bitcast.3, f32[6,5]{1,0:T(8,128)} %bias_hbm.1), custom_call_target="tpu_custom_call" | custom-call | tf_op jit(solution)/shard_map/pallas_call | solution.py:250
  22.0 1.7 %shard_map.69 = (bf16[3,8,64,128]{3,2,1,0:T(8,128)(2,1)}, bf16[3,320]{1,0:T(4,128)(2,1)}) custom-call(bf16[8,64,384]{2,1,0:T(8,128)(2,1)S(1)} %get-tuple-element.4.recv, f32[4,8,24,128]{3,2,1,0:T(8,128)S(1)} %get-tuple-element.5.msg), custom_call_target="tpu_custom_call" | custom-call | tf_op jit(solution)/shard_map/pallas_call | solution.py:277

commit v3 on v2

--- a/solution.py
+++ b/solution.py
@@ -22,6 +22,10 @@
             index = index + (1 - 2 * ((index // bit) % 2)) * bit
         bit *= 2
     return index
+
+
+def packed_rows(pairs, group):
+    return pairs * group // 8 * 8 + 8
 
 
 def kernel(
@@ -180,7 +184,10 @@
             kv = recv[b, :, p * 2 * hd:(p + 1) * 2 * hd]
             reads.append(jnp.dot(weights[p * ROWS:(p + 1) * ROWS], kv, preferred_element_type=jnp.float32))
         read = jnp.concatenate(reads, axis=0)
-        msg[mt, b] = jnp.where(left_half, sums[:, 128:128 + 2 * hd], read)
+        both = jnp.where(left_half, sums[:, 128:128 + 2 * hd], read)
+        packed = [both[p * ROWS:p * ROWS + group] for p in range(pairs)]
+        packed.append(jnp.zeros((packed_rows(pairs, group) - pairs * group, 2 * hd), jnp.float32))
+        msg[mt, b] = jnp.concatenate(packed, axis=0)
         for t in range(1, tp):
             msg_copy(b, lax.rem(mt + t, tp)).start()
 
@@ -202,7 +209,7 @@
             msg_copy(b, lax.rem(mt + t, tp)).wait_send()
 
 
-def finish(sp, tp, hd, group, pairs, recv, msg, stored_hbm, first_ref, fin, out_sem):
+def finish(sp, tp, hd, group, pairs, recv, msg, stored_hbm, first_hbm, fin, first_v, out_sem, first_sem):
     copies = [
         pltpu.make_async_copy(recv.at[b, :, pl.ds(p * 2 * hd, 2 * hd)], stored_hbm.at[p, b], out_sem.at[b, p])
         for b in range(sp)
@@ -210,7 +217,7 @@
     ]
     for copy in copies:
         copy.start()
-    left_half = lax.broadcasted_iota(jnp.int32, (pairs * ROWS, 2 * hd), 1) < hd
+    left_half = lax.broadcasted_iota(jnp.int32, (packed_rows(pairs, group), 2 * hd), 1) < hd
 
     def add_block(i, carry):
         total, acc = carry
@@ -221,16 +228,19 @@
             acc = acc + pltpu.roll(m, hd, 1)
         return total, acc
 
-    zero = jnp.zeros((pairs * ROWS, 2 * hd), jnp.float32)
+    zero = jnp.zeros((packed_rows(pairs, group), 2 * hd), jnp.float32)
     total, _ = lax.fori_loop(0, sp, add_block, (zero, zero), unroll=True)
     total = jnp.where(left_half, 0.0, total)
     squares = jnp.sum(total * total, axis=1, keepdims=True) * (1.0 / hd)
     fin[...] = pltpu.roll(total * lax.rsqrt(squares + EPS_NORM), hd, 1)
-    cols = [fin[pl.ds(g, pairs, stride=ROWS), :][:, :hd] for g in range(group)]
-    first_ref[...] = jnp.concatenate(cols, axis=1).astype(first_ref.dtype)
+    cols = [fin[pl.ds(g, pairs, stride=group), :][:, :hd] for g in range(group)]
+    first_v[...] = jnp.concatenate(cols, axis=1).astype(first_v.dtype)
+    first_copy = pltpu.make_async_copy(first_v, first_hbm, first_sem)
+    first_copy.start()
 
     for copy in copies:
         copy.wait()
+    first_copy.wait()
 
 
 def solution(mesh):
@@ -244,14 +254,14 @@
         block = pairs * 2 * hd
         any_spec = pl.BlockSpec(memory_space=pltpu.HBM)
         dma = pltpu.SemaphoreType.DMA
-        handed = sp * sub * block * 2 + tp * sp * pairs * ROWS * 2 * hd * 4
+        handed = sp * sub * block * 2 + tp * sp * packed_rows(pairs, group) * 2 * hd * 4
         limit = VMEM_BYTES - handed
         vmem_spec = pl.BlockSpec(memory_space=pltpu.VMEM)
         recv, msg = pl.pallas_call(
             functools.partial(kernel, sp, tp, seqs, sub, hd, kvh, group, pairs),
             out_shape=(
                 pltpu.VMEM((sp, sub, block), jnp.bfloat16),
-                pltpu.VMEM((tp, sp, pairs * ROWS, 2 * hd), jnp.float32),
+                pltpu.VMEM((tp, sp, packed_rows(pairs, group), 2 * hd), jnp.float32),
             ),
             in_specs=[any_spec] * 5,
             out_specs=(vmem_spec, vmem_spec),
@@ -281,10 +291,12 @@
                 jax.ShapeDtypeStruct((pairs, group * hd), jnp.bfloat16),
             ),
             in_specs=[vmem_spec, vmem_spec],
-            out_specs=(any_spec, vmem_spec),
+            out_specs=(any_spec, any_spec),
             scratch_shapes=[
-                pltpu.VMEM((pairs * ROWS, 2 * hd), jnp.float32),
+                pltpu.VMEM((packed_rows(pairs, group), 2 * hd), jnp.float32),
+                pltpu.VMEM((pairs, group * hd), jnp.bfloat16),
                 dma((sp, pairs)),
+                dma(()),
             ],
             compiler_params=pltpu.CompilerParams(vmem_limit_bytes=VMEM_BYTES // 4),
         )(recv, msg)

time: 23.9 us -> 23.3 us (0.975)
  Pallas kernels: 23.1 us -> 22.6 us
    pallas_call x1, Pallas kernels: 1.67 us -> 1.18 us  [per_device(): pl.pallas_call(functools.partial(finish, sp, tp, hd, group, pairs), out_s...]
where the time goes in v3:
time: 23.3 us; the launch traced here: 23.2 us
  Pallas kernels  22.6 us (97%)
  between operations  0.64 us (3%)
    pallas_call x1, Pallas kernels, per_device(): pl.pallas_call(functools.partial(kernel, sp, tp, seqs, sub, hd, kvh, grou...  21.4 us
    pallas_call x1, Pallas kernels, per_device(): pl.pallas_call(functools.partial(finish, sp, tp, hd, group, pairs), out_s...  1.18 us

profile of v3, /device:TPU:0, one launch (start us, length us, event | category | flops | bytes accessed | tf_op | source)
XLA Modules:
  0.0 23.2 jit_solution(2777795945533988560)
XLA Ops:
  0.6 21.4 %shard_map.68 = (bf16[8,64,384]{2,1,0:T(8,128)(2,1)S(1)}, f32[4,8,16,128]{3,2,1,0:T(8,128)S(1)}) custom-call(bf16[256,2048]{1,0:T(8,128)(2,1)} %bitcast.2, bf16[2048,384]{1,0:T(8,128)(2,1)} %wk_hbm.1, bf16[2048,384]{1,0:T(8,128)(2,1)} %wv_hbm.1, bf16[5,3,64]{2,1,0:T(4,128)(2,1)} %bitcast.3, f32[6,5]{1,0:T(8,128)} %bias_hbm.1), custom_call_target="tpu_custom_call" | custom-call | tf_op jit(solution)/shard_map/pallas_call | solution.py:260
  22.0 1.2 %shard_map.69 = (bf16[3,8,64,128]{3,2,1,0:T(8,128)(2,1)}, bf16[3,320]{1,0:T(4,128)(2,1)}) custom-call(bf16[8,64,384]{2,1,0:T(8,128)(2,1)S(1)} %get-tuple-element.4.recv, f32[4,8,16,128]{3,2,1,0:T(8,128)S(1)} %get-tuple-element.5.msg), custom_call_target="tpu_custom_call" | custom-call | tf_op jit(solution)/shard_map/pallas_call | solution.py:287
